TPU v7x, 32 devices: a whole 2x2x4 slice. The times are simulated.
32 devices in a mesh: sp: 4 (over y, x), tp: 8 (over z, core).
Axes of the slice: x: 2, y: 2, z: 4, core: 2. Of those that a mesh axis runs over, the one named last changes fastest.
Arguments:
- moe_input: bfloat16 [512, 2048], P('sp'), may hold values from -6 to 6
- cotangent: bfloat16 [512, 2048], P('sp'), may hold values from -6 to 6
- route_expert: int32 [512, 2], P('sp'), may hold values from 0 to 3, all different within a row; in each aligned block of 128 rows (0 to 127, 128 to 255, ...) at most 128 rows name the same one
- route_weight: float32 [512, 2], P('sp'), may hold values from 0.2 to 1
- w_gate: bfloat16 [4, 2048, 6144], P('sp', None, 'tp'), may hold values from -0.125 to 0.125
- w_up: bfloat16 [4, 2048, 6144], P('sp', None, 'tp'), may hold values from -0.125 to 0.125
- w_down: bfloat16 [4, 6144, 2048], P('sp', 'tp'), may hold values from -0.078125 to 0.078125
- out_proj: bfloat16 [2048, 2048], P('tp'), may hold values from -0.125 to 0.125
- saved_out: bfloat16 [512, 2048], P('sp', 'tp'), may hold values from -6 to 6
- queries: bfloat16 [512, 1024], P('sp', 'tp'), may hold values from -6 to 6
- keys: bfloat16 [512, 1024], P('sp', 'tp'), may hold values from -6 to 6
- values: bfloat16 [512, 2048], P('sp', 'tp'), may hold values from -6 to 6
- log_decay: float32 [512, 1024], P('sp', 'tp'), may hold values from -1 to 0
- span_state: float32 [8, 1024, 128], P('sp', 'tp'), may hold values from -6 to 6
Outputs:
- grad_w_gate: bfloat16 [4, 2048, 6144], P('sp', None, 'tp')
- grad_w_up: bfloat16 [4, 2048, 6144], P('sp', None, 'tp')
- grad_w_down: bfloat16 [4, 6144, 2048], P('sp', 'tp')
- grad_proj: float32 [2048, 2048], P('sp', 'tp')
- grad_queries: bfloat16 [512, 1024], P('sp', 'tp')
- grad_keys: bfloat16 [512, 1024], P('sp', 'tp')
- grad_values: bfloat16 [512, 2048], P('sp', 'tp')
- grad_decay: float32 [512, 1024], P('sp', 'tp')
Inputs may be any that keep to these rules, and one draw needn't show every extreme that they name: `route_expert`: each row names two different experts. Within the 128 rows of one index of sp no expert is named by more than 128 rows, a bound that some block reaches.
All inputs are finite; a program needn't handle non-finite values.
Results may differ from a plain program's by a relative error of at most 0.019.
Values may be sent and summed in bfloat16 or wider, within the bound.
No kernel may reach another device: no remote copies, remote signals or barrier semaphores. Data moves between devices by JAX's collectives and lax.ppermute only.
A program may use at most 128 MiB of HBM per device.

v0:
```python
import jax
import jax.numpy as jnp
from jax import lax
from jax.sharding import PartitionSpec as P

DK = 64
SPAN = 64
HIGH = lax.Precision.HIGHEST


def entering(shard, axis, combine, identity):
    length, mine = (lax.axis_size(axis), lax.axis_index(axis))
    everything = jax.tree.map(lambda part: lax.all_gather(part, axis), shard)
    start = jax.tree.map(
        lambda part, zero: jnp.broadcast_to(jnp.asarray(zero, part.dtype), part.shape),
        shard,
        identity,
    )

    def step(k, before):
        at = length - 1 - k
        reached = at > mine
        new = combine(before, jax.tree.map(lambda part: part[at], everything))
        return jax.tree.map(lambda a, b: jnp.where(reached, a, b), new, before)

    return lax.fori_loop(0, length, step, start)


def slot_places(experts, count):
    routes_flat = experts.reshape(-1)
    one_hot = (routes_flat[:, None] == jnp.arange(count, dtype=jnp.int32)[None, :]).astype(
        jnp.int32
    )
    earlier = jnp.cumsum(one_hot, axis=0) - one_hot
    return jnp.sum(earlier * one_hot, axis=1).reshape(experts.shape)


def expert_grads(inputs, routed, gate_weight, up_weight, down_weight):
    gate = jnp.dot(inputs, gate_weight, preferred_element_type=jnp.float32)
    upper = jnp.dot(inputs, up_weight, preferred_element_type=jnp.float32)
    sigmoid_gate = jax.nn.sigmoid(gate)
    active = gate * sigmoid_gate
    hidden = (active * upper).astype(jnp.bfloat16)
    d_hidden = lax.dot_general(
        routed, down_weight, (((1,), (1,)), ((), ())), preferred_element_type=jnp.float32
    )
    d_upper = (d_hidden * active).astype(jnp.bfloat16)
    d_gate = (d_hidden * upper * sigmoid_gate * (1.0 + gate * (1.0 - sigmoid_gate))).astype(
        jnp.bfloat16
    )
    grad_down = lax.dot_general(
        hidden, routed, (((0,), (0,)), ((), ())), preferred_element_type=jnp.float32
    ).astype(jnp.bfloat16)
    grad_gate = lax.dot_general(
        inputs, d_gate, (((0,), (0,)), ((), ())), preferred_element_type=jnp.float32
    ).astype(jnp.bfloat16)
    grad_up = lax.dot_general(
        inputs, d_upper, (((0,), (0,)), ((), ())), preferred_element_type=jnp.float32
    ).astype(jnp.bfloat16)
    return (d_gate, d_upper, grad_gate, grad_up, grad_down)


def input_grad(d_gate, d_upper, gate_weight, up_weight):
    first = lax.dot_general(
        d_gate, gate_weight, (((1,), (1,)), ((), ())), preferred_element_type=jnp.float32
    )
    second = lax.dot_general(
        d_upper, up_weight, (((1,), (1,)), ((), ())), preferred_element_type=jnp.float32
    )
    return first + second


def gated_pieces(queries, keys, values, log_decay, grad_mix, key_dim, span_len):
    value_dim = values.shape[1] * key_dim // queries.shape[1]
    heads = queries.shape[1] // key_dim
    spans = queries.shape[0] // span_len

    def blocks(array, width):
        return array.astype(jnp.float32).reshape(spans, span_len, heads, width)

    query_spans = blocks(queries, key_dim)
    key_spans = blocks(keys, key_dim)
    value_spans = blocks(values, value_dim)
    grad_spans = blocks(grad_mix, value_dim)
    cumulative = jnp.cumsum(blocks(log_decay, key_dim), axis=1)
    last = cumulative[:, -1]
    scale = key_dim ** (-0.5)
    query_decayed = query_spans * jnp.exp(cumulative)
    key_grown = key_spans * jnp.exp(-cumulative)
    key_to_end = key_spans * jnp.exp(last[:, None] - cumulative)
    g_local = scale * jnp.einsum("nthk,nthv->nhkv", query_decayed, grad_spans, precision=HIGH)
    return (
        query_spans,
        key_spans,
        value_spans,
        grad_spans,
        cumulative,
        last,
        query_decayed,
        key_grown,
        key_to_end,
        g_local,
    )


def backward_step(carry, inputs):
    local, decay = inputs
    return (local + jnp.exp(decay)[..., None] * carry, carry)


def gated_finish(pieces, span_state, g_end, key_dim):
    (
        query_spans,
        key_spans,
        value_spans,
        grad_spans,
        cumulative,
        last,
        query_decayed,
        key_grown,
        key_to_end,
        g_local,
    ) = pieces
    spans, span_len, heads, value_dim = value_spans.shape
    scale = key_dim ** (-0.5)
    token_locations = jnp.arange(span_len, dtype=jnp.int32)
    causal = (token_locations[:, None] >= token_locations[None, :]).astype(jnp.float32)
    scores = jnp.einsum("nthk,nshk->nhts", query_decayed, key_grown, precision=HIGH) * causal
    grad_dot = jnp.einsum("nthv,nshv->nhts", grad_spans, value_spans, precision=HIGH) * causal
    state = span_state.reshape(spans, heads, key_dim, value_dim)
    d_query = (
        scale
        * jnp.exp(cumulative)
        * (
            jnp.einsum("nhts,nshk->nthk", grad_dot, key_grown, precision=HIGH)
            + jnp.einsum("nthv,nhkv->nthk", grad_spans, state, precision=HIGH)
        )
    )
    d_key = scale * jnp.exp(-cumulative) * jnp.einsum(
        "nhts,nthk->nshk", grad_dot, query_decayed, precision=HIGH
    ) + jnp.exp(last[:, None] - cumulative) * jnp.einsum(
        "nshv,nhkv->nshk", value_spans, g_end, precision=HIGH
    )
    d_value = scale * jnp.einsum(
        "nhts,nthv->nshv", scores, grad_spans, precision=HIGH
    ) + jnp.einsum("nshk,nhkv->nshv", key_to_end, g_end, precision=HIGH)
    state_end = jnp.exp(last)[..., None] * state + jnp.einsum(
        "nshk,nshv->nhkv", key_to_end, value_spans, precision=HIGH
    )
    tail = jnp.sum(state_end * g_end, axis=-1)
    d_cumulative = query_spans * d_query - key_spans * d_key
    d_log = jnp.cumsum(d_cumulative[:, ::-1], axis=1)[:, ::-1] + tail[:, None]
    rows = spans * span_len
    return (
        d_query.reshape(rows, heads * key_dim).astype(jnp.bfloat16),
        d_key.reshape(rows, heads * key_dim).astype(jnp.bfloat16),
        d_value.reshape(rows, heads * value_dim).astype(jnp.bfloat16),
        d_log.reshape(rows, heads * key_dim),
    )


def carry_combine(earlier, later):
    return (later[0] * earlier[0], later[1] + later[0][..., None] * earlier[1])


def on_device(
    moe_input,
    cotangent,
    route_expert,
    route_weight,
    w_gate,
    w_up,
    w_down,
    out_proj,
    saved_out,
    queries,
    keys,
    values,
    log_decay,
    span_state,
):
    tok_rows, width = moe_input.shape
    groups = lax.axis_size("sp")
    lanes = lax.axis_size("tp")
    capacity = 4 * tok_rows // groups
    target_locations = slot_places(route_expert, groups)
    rows_index = (target_locations * groups + route_expert).reshape(-1)
    owner = (
        jnp.full((capacity * groups,), 2 * tok_rows, jnp.int32)
        .at[rows_index]
        .set(jnp.arange(2 * tok_rows, dtype=jnp.int32))
    )
    weighted = (route_weight[:, :, None] * cotangent[:, None, :].astype(jnp.float32)).astype(
        jnp.bfloat16
    )
    weighted = weighted.reshape(2 * tok_rows, width)
    blank = jnp.zeros((1, width), jnp.bfloat16)
    send_in = jnp.concatenate([moe_input, blank], axis=0)[owner // 2].reshape(
        capacity, groups, width
    )
    send_cot = jnp.concatenate([weighted, blank], axis=0)[owner].reshape(capacity, groups, width)
    gate_weight = w_gate[0]
    up_weight = w_up[0]
    down_weight = w_down[0]
    share = capacity // lanes
    lane = lax.axis_index("tp")
    part_in = lax.dynamic_slice_in_dim(send_in, lane * share, share, 0)
    part_cot = lax.dynamic_slice_in_dim(send_cot, lane * share, share, 0)
    got_in, got_cot = (
        lax.all_to_all(part_in, "sp", split_axis=1, concat_axis=1, tiled=True),
        lax.all_to_all(part_cot, "sp", split_axis=1, concat_axis=1, tiled=True),
    )
    full_in, full_cot = (
        lax.all_gather(got_in, "tp", axis=0, tiled=True),
        lax.all_gather(got_cot, "tp", axis=0, tiled=True),
    )
    d_gate, d_upper, grad_gate, grad_up, grad_down = expert_grads(
        full_in.reshape(-1, width), full_cot.reshape(-1, width), gate_weight, up_weight, down_weight
    )
    mine = (
        lax.psum_scatter(
            input_grad(d_gate, d_upper, gate_weight, up_weight).astype(jnp.bfloat16),
            "tp",
            scatter_dimension=0,
            tiled=True,
        )
        .astype(jnp.float32)
        .reshape(share, groups, width)
    )
    returned = (
        lax.all_to_all(mine.astype(jnp.bfloat16), "sp", split_axis=1, concat_axis=1, tiled=True)
        .astype(mine.dtype)
        .reshape(-1, width)
    )
    local_index = rows_index - lane * share * groups
    inside = (local_index >= 0) & (local_index < share * groups)
    picked = jnp.where(inside[:, None], returned[jnp.clip(local_index, 0, share * groups - 1)], 0.0)
    routed = jnp.sum(picked.reshape(tok_rows, 2, width), axis=1)
    total = lax.psum(routed.astype(jnp.bfloat16), "tp").astype(jnp.float32)
    grad_in = (cotangent.astype(jnp.float32) + total).astype(jnp.bfloat16)
    grad_mix = lax.dot_general(
        grad_in, out_proj, (((1,), (1,)), ((), ())), preferred_element_type=jnp.float32
    )
    grad_proj = lax.psum_scatter(
        lax.dot_general(
            grad_in, saved_out, (((0,), (0,)), ((), ())), preferred_element_type=jnp.float32
        ).astype(jnp.bfloat16),
        "sp",
        scatter_dimension=0,
        tiled=True,
    ).astype(jnp.float32)
    pieces = gated_pieces(queries, keys, values, log_decay, grad_mix, DK, SPAN)
    g_local = pieces[9]
    last = pieces[5]
    begin = jnp.zeros(g_local.shape[1:], jnp.float32)
    device_start, local_end = lax.scan(backward_step, begin, (g_local, last), reverse=True)
    device_decay = jnp.exp(jnp.sum(last, axis=0))
    identity = (jnp.ones_like(device_decay), jnp.zeros_like(device_start))
    decay_after, state_after = entering((device_decay, device_start), "sp", carry_combine, identity)
    running = jnp.cumsum(last, axis=0)
    beyond = running[-1][None] - running
    g_end = local_end + jnp.exp(beyond)[..., None] * state_after[None]
    grad_queries, grad_keys, grad_values, grad_decay = gated_finish(pieces, span_state, g_end, DK)
    return (
        grad_gate[None],
        grad_up[None],
        grad_down[None],
        grad_proj,
        grad_queries,
        grad_keys,
        grad_values,
        grad_decay,
    )


def solution(mesh):
    placed = (
        P("sp", None),
        P("sp", None),
        P("sp", None),
        P("sp", None),
        P("sp", None, "tp"),
        P("sp", None, "tp"),
        P("sp", "tp", None),
        P("tp", None),
        P("sp", "tp"),
        P("sp", "tp"),
        P("sp", "tp"),
        P("sp", "tp"),
        P("sp", "tp"),
        P("sp", "tp", None),
    )
    return jax.shard_map(
        on_device,
        mesh=mesh,
        in_specs=placed,
        out_specs=(
            P("sp", None, "tp"),
            P("sp", None, "tp"),
            P("sp", "tp", None),
            P("sp", "tp"),
            P("sp", "tp"),
            P("sp", "tp"),
            P("sp", "tp"),
            P("sp", "tp"),
        ),
        check_vma=False,
    )
```

profile of v0, /device:TPU:0, one launch (start us, length us, event | category | flops | bytes accessed | tf_op | source)
XLA Modules:
  0.0 273.4 jit_solution(1842844893253880070)
XLA Ops:
  8.5 1.2 reduce-window.6
  11.3 1.4 scatter_custom_fusion
  12.7 1.9 concatenate.6
  14.6 6.3 %gather_fusion = bf16[512,2048]{1,0:T(8,128)(2,1)} fusion(bf16[129,2048]{1,0:T(8,128)(2,1)} %concatenate.6, s32[1024]{0:T(1024)S(1)} %get-tuple-element.318), kind=kCustom, calls=%fused_computation | custom fusion | bytes 4196352 | tf_op jit(solution)/shard_map/gather | solution.py:198
  21.0 4.1 %reshape.208 = bf16[128,4,2048]{2,1,0:T(4,128)(2,1)} reshape(bf16[512,2048]{1,0:T(8,128)(2,1)} %gather_fusion) | data formatting | bytes 4194304 | tf_op jit(solution)/shard_map/reshape | solution.py:198
  25.1 1.0 constant_dynamic-slice_fusion.1
  26.3 10.7 %all_to_all.15 = bf16[16,4,2048]{2,0,1:T(8,128)(2,1)S(1)} all-to-all(bf16[16,4,2048]{2,0,1:T(8,128)(2,1)S(1)} %copy.146), channel_id=1, replica_groups=mesh['sp'=4,'tp'=8] {'sp'}, dimensions={1} | all-to-all | bytes 524288 | tf_op jit(solution)/shard_map/all_to_all | solution.py:210
  38.0 3.4 %mul.203 = f32[128,2,2048]{2,1,0:T(2,128)} broadcast(bf16[128,2048]{1,0:T(8,128)(2,1)} %param.19), dimensions={0,2} | broadcast | bytes 2621440 | tf_op jit(solution)/shard_map/mul | solution.py:193
  41.4 3.7 %mul.204 = f32[256,2048]{1,0:T(8,128)} reshape(f32[128,2,2048]{2,1,0:T(2,128)} %mul.203) | data formatting | bytes 4194304 | tf_op jit(solution)/shard_map/mul | solution.py:193
  45.3 1.9 multiply_convert_fusion
  47.2 1.1 concatenate.7
  48.3 6.6 %gather_fusion.1 = bf16[512,2048]{1,0:T(8,128)(2,1)} fusion(bf16[257,2048]{1,0:T(8,128)(2,1)} %concatenate.7, s32[1024]{0:T(1024)S(1)} %get-tuple-element.317), kind=kCustom, calls=%fused_computation.1 | custom fusion | bytes 4196352 | tf_op jit(solution)/shard_map/gather | solution.py:201
  54.9 4.1 %reshape.210 = bf16[128,4,2048]{2,1,0:T(4,128)(2,1)} reshape(bf16[512,2048]{1,0:T(8,128)(2,1)} %gather_fusion.1) | data formatting | bytes 4194304 | tf_op jit(solution)/shard_map/reshape | solution.py:201
  59.0 1.0 constant_dynamic-slice_fusion
  60.2 8.1 %all_to_all.16 = bf16[16,4,2048]{2,0,1:T(8,128)(2,1)S(1)} all-to-all(bf16[16,4,2048]{2,0,1:T(8,128)(2,1)S(1)} %copy.147), channel_id=1, replica_groups=mesh['sp'=4,'tp'=8] {'sp'}, dimensions={1} | all-to-all | bytes 524288 | tf_op jit(solution)/shard_map/all_to_all | solution.py:211
  69.5 3.9 %reshape.209 = bf16[512,2048]{1,0:T(8,128)(2,1)} reshape(bf16[128,4,2048]{2,1,0:T(4,128)(2,1)} %all-gather.6.cloned.1.call-done) | data formatting | bytes 4194304 | tf_op jit(solution)/shard_map/reshape | solution.py:218
  73.5 4.7 %fusion.3 = f32[512,768]{1,0:T(8,128)} fusion(bf16[512,2048]{1,0:T(8,128)(2,1)} %reshape.209, bf16[1,2048,768]{2,1,0:T(8,128)(2,1)S(1)} %copy-done), kind=kOutput, calls=%fused_computation.16 | convolution fusion | flops 1610612736 | bytes 6815744 | tf_op jit(solution)/shard_map/dot_general | solution.py:39
  78.2 2.9 %fusion.7 = f32[512,768]{1,0:T(8,128)} fusion(bf16[512,2048]{1,0:T(8,128)(2,1)S(1)} %copy-done.4, bf16[1,2048,768]{2,1,0:T(8,128)(2,1)S(1)} %copy-done.17), kind=kOutput, calls=%fused_computation.20 | convolution fusion | flops 1610612736 | bytes 6815744 | tf_op jit(solution)/shard_map/dot_general | solution.py:40
  81.1 17.2 %all-gather.8.cloned.1.call-done = bf16[128,4,2048]{2,1,0:T(4,128)(2,1)} async-done(((bf16[16,4,2048]{2,1,0:T(4,128)(2,1)}), bf16[128,4,2048]{2,1,0:T(4,128)(2,1)}) %all-gather.8.cloned.1.call-update) | async-done | bytes 2097168 | tf_op jit(solution)/shard_map/all_gather | solution.py:215
  98.3 3.9 %reshape.211 = bf16[512,2048]{1,0:T(8,128)(2,1)} reshape(bf16[128,4,2048]{2,1,0:T(4,128)(2,1)} %all-gather.8.cloned.1.call-done) | data formatting | bytes 4194304 | tf_op jit(solution)/shard_map/reshape | solution.py:218
  102.3 5.6 %multiply_convert_fusion.2 = (bf16[512,768]{1,0:T(8,128)(2,1)S(1)}, bf16[512,768]{1,0:T(8,128)(2,1)S(1)}) fusion(f32[512,768]{1,0:T(8,128)} %fusion.3, f32[512,768]{1,0:T(8,128)} %fusion.7, bf16[512,2048]{1,0:T(8,128)(2,1)} %reshape.211, bf16[1,768,2048]{2,1,0:T(8,128)(2,1)} %param.24), kind=kOutput, calls=%fused_computation.31 | convolution fusion | flops 1615724544 | bytes 9961472 | tf_op jit(solution)/shard_map/dot_general | solution.py:44
  107.9 1.8 fusion.1
  110.4 3.2 %add_convert_fusion = bf16[512,2048]{1,0:T(8,128)(2,1)} fusion(f32[512,2048]{1,0:T(8,128)S(1)} %fusion.1, bf16[512,768]{1,0:T(8,128)(2,1)S(1)} %get-tuple-element.305, bf16[1,2048,768]{2,1,0:T(8,128)(2,1)S(1)} %copy-done.18), kind=kOutput, calls=%fused_computation.10 | convolution fusion | flops 1612709888 | bytes 10223616 | tf_op jit(solution)/shard_map/dot_general | solution.py:67
  115.3 8.0 %all-gather.2 = f32[4,2,64]{2,1,0:T(2,128)S(1)} all-gather(f32[1,2,64]{2,1,0:T(2,128)S(1)} %exponential_bitcast_fusion.1), channel_id=3, replica_groups=mesh['sp'=4,'tp'=8] {'sp'}, dimensions={0}, use_global_device_ids=true | all-gather | bytes 2560 | tf_op jit(solution)/shard_map/all_gather | solution.py:13
  123.4 1.1 convolution_multiply_fusion.2
  124.4 6.3 %fusion.13 = bf16[1,768,2048]{2,1,0:T(8,128)(2,1)} fusion(bf16[512,2048]{1,0:T(8,128)(2,1)} %reshape.211, f32[512,768]{1,0:T(8,128)} %fusion.7, f32[512,768]{1,0:T(8,128)} %fusion.3), kind=kOutput, calls=%fused_computation.26 | convolution fusion | flops 1614544896 | bytes 8388608 | tf_op jit(solution)/shard_map/dot_general | solution.py:51
  130.7 18.3 %reduce-scatter.3.cloned.1.call-done = bf16[64,2048]{1,0:T(8,128)(2,1)} async-done(((bf16[512,2048]{1,0:T(8,128)(2,1)}), bf16[64,2048]{1,0:T(8,128)(2,1)}) %reduce-scatter.3.cloned.1.call-update) | async-done | bytes 262160 | tf_op jit(solution)/shard_map/reduce_scatter | solution.py:221
  149.0 1.1 convert_element_type.102
  150.9 3.8 %all-to-all-start.2 = ((bf16[16,4,2048]{2,0,1:T(8,128)(2,1)}), bf16[16,4,2048]{2,0,1:T(8,128)(2,1)S(1)}, u32[]{:S(2)}, u32[]{:S(2)}) async-start(bf16[16,4,2048]{2,0,1:T(8,128)(2,1)} %copy.115), calls=%async_computation.3 | async-start | bytes 524288 | tf_op jit(solution)/shard_map/all_to_all | solution.py:231
  154.7 4.6 %fusion.12 = bf16[1,2048,768]{2,1,0:T(8,128)(2,1)} fusion(bf16[512,2048]{1,0:T(8,128)(2,1)S(1)} %copy-done.5, bf16[512,768]{1,0:T(8,128)(2,1)} %copy-done.19), kind=kOutput, calls=%fused_computation.25 | convolution fusion | flops 1612185600 | bytes 6029312 | tf_op jit(solution)/shard_map/dot_general | solution.py:57
  160.5 1.5 gather_fusion.2
  161.9 2.3 gather.14
  164.2 5.8 %select_reduce_fusion = bf16[128,2048]{1,0:T(8,128)(2,1)} fusion(f32[128,2,2048]{2,1,0:T(2,128)} %gather.14, pred[128,2]{1,0:T(8,128)(4,1)S(1)} %copy.114), kind=kLoop, calls=%fused_computation.28 | loop fusion | flops 786432 | bytes 2621696 | tf_op jit(solution)/shard_map/reduce_sum | solution.py:238
  170.2 4.7 %fusion.11 = bf16[1,2048,768]{2,1,0:T(8,128)(2,1)} fusion(bf16[512,2048]{1,0:T(8,128)(2,1)S(1)} %copy-done.6, bf16[512,768]{1,0:T(8,128)(2,1)} %copy-done.20), kind=kOutput, calls=%fused_computation.24 | convolution fusion | flops 1612185600 | bytes 6029312 | tf_op jit(solution)/shard_map/dot_general | solution.py:54
  174.9 49.9 %all-reduce.4.cloned.1.call-done = bf16[128,2048]{1,0:T(8,128)(2,1)} async-done(((bf16[128,2048]{1,0:T(8,128)(2,1)}), bf16[128,2048]{1,0:T(8,128)(2,1)}) %all-reduce.4.cloned.1.call-update) | async-done | bytes 524304 | tf_op jit(solution)/shard_map/psum | solution.py:239
  224.7 1.9 fusion.27
  227.4 9.5 %all-gather = f32[8,64,128]{2,1,0:T(8,128)S(1)} all-gather(f32[2,64,128]{2,1,0:T(8,128)S(1)} %get-tuple-element.245), channel_id=2, replica_groups=mesh['sp'=4,'tp'=8] {'sp'}, dimensions={0}, use_global_device_ids=true | all-gather | bytes 327680 | tf_op jit(solution)/shard_map/all_gather | solution.py:13
  237.5 1.4 convolution_convert_fusion.3
  240.2 1.0 multiply_subtract_fusion
  241.2 1.8 rev.6
  243.0 1.7 copy.139
  244.7 1.3 fusion.24
  246.1 1.0 fusion.57
  247.8 1.7 reshape.222
  249.4 1.4 convolution_multiply_fusion.1
  250.8 1.4 fusion.25
  255.4 9.7 %reduce-scatter.5.cloned.1.call-done = bf16[512,256]{1,0:T(8,128)(2,1)} async-done(((bf16[2048,256]{1,0:T(8,128)(2,1)}), bf16[512,256]{1,0:T(8,128)(2,1)}) %reduce-scatter.5.cloned.1.call-update) | async-done | bytes 262160 | tf_op jit(solution)/shard_map/reduce_scatter | solution.py:244
  265.1 1.8 convert_element_type.107
  (133 shorter events, 16.9 us)
Async XLA Ops:
  7.2 66.3 %copy-start = (bf16[1,2048,768]{2,1,0:T(8,128)(2,1)S(1)}, bf16[1,2048,768]{2,1,0:T(8,128)(2,1)}, u32[]{:S(2)}) copy-start(bf16[1,2048,768]{2,1,0:T(8,128)(2,1)} %param.22) | copy-start | bytes 9437188
  7.2 62.3 %all-gather.6.cloned.1.call-start = ((), (), s32[]{:S(2)}) async-start(), calls=%async_computation.5 | async-start | bytes 2359296 | tf_op jit(solution)/shard_map/all_gather | solution.py:214
  38.0 60.4 %all-gather.8.cloned.1.call-start = ((), (), s32[]{:S(2)}) async-start(), calls=%async_computation.6 | async-start | bytes 2359296 | tf_op jit(solution)/shard_map/all_gather | solution.py:215
  41.4 3.7 %copy-start.16 = (f32[128,2]{0,1:T(2,128)S(1)}, f32[128,2]{0,1:T(2,128)}, u32[]{:S(2)}) copy-start(f32[128,2]{0,1:T(2,128)} %param.21) | copy-start | bytes 3076
  69.3 79.7 %reduce-scatter.3.cloned.1.call-start = ((), (), s32[]{:S(2)}) async-start(), calls=%async_computation.7 | async-start | bytes 2359296 | tf_op jit(solution)/shard_map/reduce_scatter | solution.py:221
  73.5 4.7 %copy-start.4 = (bf16[512,2048]{1,0:T(8,128)(2,1)S(1)}, bf16[512,2048]{1,0:T(8,128)(2,1)}, u32[]{:S(2)}) copy-start(bf16[512,2048]{1,0:T(8,128)(2,1)} %reshape.209) | copy-start | bytes 6291460
  73.5 4.7 %copy-start.17 = (bf16[1,2048,768]{2,1,0:T(8,128)(2,1)S(1)}, bf16[1,2048,768]{2,1,0:T(8,128)(2,1)}, u32[]{:S(2)}) copy-start(bf16[1,2048,768]{2,1,0:T(8,128)(2,1)} %param.23) | copy-start | bytes 9437188
  107.9 1.9 copy-start.20
  107.9 1.9 copy-start.19
  107.9 2.5 copy-start.18
  113.6 0.8 copy-start.11
  113.6 1.2 copy-start.14
  113.6 1.4 copy-start.15
  113.6 1.7 copy-start.13
  124.4 30.3 %copy-start.5 = (bf16[512,2048]{1,0:T(8,128)(2,1)S(1)}, bf16[512,2048]{1,0:T(8,128)(2,1)}, u32[]{:S(2)}) copy-start(bf16[512,2048]{1,0:T(8,128)(2,1)} %reshape.209) | copy-start | bytes 6291460
  150.9 9.2 %all-to-all-start.2 = ((bf16[16,4,2048]{2,0,1:T(8,128)(2,1)}), bf16[16,4,2048]{2,0,1:T(8,128)(2,1)S(1)}, u32[]{:S(2)}, u32[]{:S(2)}) async-start(bf16[16,4,2048]{2,0,1:T(8,128)(2,1)} %copy.115), calls=%async_computation.3 | async-start | bytes 524288 | tf_op jit(solution)/shard_map/all_to_all | solution.py:231
  154.7 70.0 %all-reduce.4.cloned.1.call-start = ((), (), s32[]{:S(2)}) async-start(), calls=%async_computation.8 | async-start | bytes 1048576 | tf_op jit(solution)/shard_map/psum | solution.py:239
  164.2 5.9 %copy-start.6 = (bf16[512,2048]{1,0:T(8,128)(2,1)S(1)}, bf16[512,2048]{1,0:T(8,128)(2,1)}, u32[]{:S(2)}) copy-start(bf16[512,2048]{1,0:T(8,128)(2,1)} %reshape.209) | copy-start | bytes 6291460
  170.1 54.6 %copy-start.2 = (bf16[128,2048]{1,0:T(8,128)(2,1)S(1)}, bf16[128,2048]{1,0:T(8,128)(2,1)}, u32[]{:S(2)}) copy-start(bf16[128,2048]{1,0:T(8,128)(2,1)} %param.19) | copy-start | bytes 1572868
  170.1 95.0 %reduce-scatter.5.cloned.1.call-start = ((), (), s32[]{:S(2)}) async-start(), calls=%async_computation.9 | async-start | bytes 1310720 | tf_op jit(solution)/shard_map/reduce_scatter | solution.py:244
  226.6 10.8 %copy-start.7 = (bf16[128,2048]{1,0:T(8,128)(2,1)S(1)}, bf16[128,2048]{1,0:T(8,128)(2,1)}, u32[]{:S(2)}) copy-start(bf16[128,2048]{1,0:T(8,128)(2,1)} %all-reduce.4.cloned.1.call-done) | copy-start | bytes 1572868
  226.6 10.8 %copy-start.12 = (bf16[128,256]{1,0:T(8,128)(2,1)S(1)}, bf16[128,256]{1,0:T(8,128)(2,1)}, u32[]{:S(2)}) copy-start(bf16[128,256]{1,0:T(8,128)(2,1)} %param.26) | copy-start | bytes 196612
  226.7 12.5 %copy-start.3 = (f32[2,64,2,128]{3,2,1,0:T(2,128)}, f32[2,64,2,128]{3,2,1,0:T(2,128)S(1)}, u32[]{:S(2)}) copy-start(f32[2,64,2,128]{3,2,1,0:T(2,128)S(1)} %reshape.217) | copy-start | bytes 393220
  227.4 12.2 %copy-start.8 = (f32[2,2,64,128]{3,2,1,0:T(8,128)}, f32[2,2,64,128]{3,2,1,0:T(8,128)S(1)}, u32[]{:S(2)}) copy-start(f32[2,2,64,128]{3,2,1,0:T(8,128)S(1)} %get-tuple-element.244) | copy-start | bytes 393220
  237.5 1.7 copy-start.9
  241.2 25.7 %copy-start.1 = (bf16[1,2048,768]{2,1,0:T(8,128)(2,1)S(1)}, bf16[1,2048,768]{2,1,0:T(8,128)(2,1)}, u32[]{:S(2)}) copy-start(bf16[1,2048,768]{2,1,0:T(8,128)(2,1)} %param.22) | copy-start | bytes 9437188
  246.1 8.5 %copy-start.10 = (bf16[2,64,2,64]{1,3,2,0:T(8,128)(2,1)S(1)}, bf16[2,64,2,64]{1,3,2,0:T(8,128)(2,1)}, u32[]{:S(2)}) copy-start(bf16[2,64,2,64]{1,3,2,0:T(8,128)(2,1)} %get-tuple-element.309) | copy-start | bytes 98308
Sparse Core Ops, SparseCore 0:
  38.1 28.8 all-gather.5
  69.4 28.8 all-gather.7
  113.7 35.2 reduce-scatter.2
  170.2 54.4 all-reduce.3
  239.1 26.0 reduce-scatter.4
where the time goes:
time: 275 us; the launch traced here: 273 us
  waiting for transfers between devices  95.9 us (35%)
  local copies, waits for them, and re-layouts  63.6 us (23%)
  matrix products  44.8 us (16%)
  blocking collectives  36.4 us (13%)
  between operations  14.4 us (5%)
  other arithmetic  14 us (5%)
  starting transfers between devices  4.16 us (2%)
    psum x1, waiting for transfers between devices, on_device(): total = lax.psum(routed.astype(jnp.bfloat16), 'tp').astype(jnp.float32)  49.9 us
    reduce_scatter x1, waiting for transfers between devices, on_device(): lax.psum_scatter(input_grad(d_gate, d_upper, gate_weight, up_weight).asty...  18.3 us
    all_gather x2, blocking collectives, entering(): everything = jax.tree.map(lambda part: lax.all_gather(part, axis), shard)  17.5 us
    all_gather x1, waiting for transfers between devices, on_device(): lax.all_gather(got_cot, 'tp', axis=0, tiled=True)  17.2 us
    all_to_all x1, blocking collectives, on_device(): lax.all_to_all(part_in, 'sp', split_axis=1, concat_axis=1, tiled=True)  10.7 us
    reduce_scatter x1, waiting for transfers between devices, on_device(): lax.psum_scatter(lax.dot_general(grad_in, saved_out, (((0,), (0,)), ((),...  9.71 us
    all_to_all x1, blocking collectives, on_device(): lax.all_to_all(part_cot, 'sp', split_axis=1, concat_axis=1, tiled=True)  8.11 us
    mul x3, local copies, waits for them, and re-layouts, on_device(): route_weight[:, :, None] * cotangent[:, None, :].astype(jnp.float32)  7.21 us
  transfers between devices with their start and end apart: 6, of which 5 were waited for; matrix products, arithmetic and copies ran while one was open for 25% of the time, Pallas kernels for 0%

commit v1 on v0

--- a/solution.py
+++ b/solution.py
@@ -6,6 +6,12 @@
 DK = 64
 SPAN = 64
 HIGH = lax.Precision.HIGHEST
+
+
+def add_all(block, name):
+    parts = lax.all_gather(block, name, axis=0, tiled=False)
+    acc = parts.sum(axis=0)
+    return acc
 
 
 def entering(shard, axis, combine, identity):
@@ -236,7 +242,7 @@
     inside = (local_index >= 0) & (local_index < share * groups)
     picked = jnp.where(inside[:, None], returned[jnp.clip(local_index, 0, share * groups - 1)], 0.0)
     routed = jnp.sum(picked.reshape(tok_rows, 2, width), axis=1)
-    total = lax.psum(routed.astype(jnp.bfloat16), "tp").astype(jnp.float32)
+    total = add_all(routed.astype(jnp.bfloat16), "tp").astype(jnp.float32)
     grad_in = (cotangent.astype(jnp.float32) + total).astype(jnp.bfloat16)
     grad_mix = lax.dot_general(
         grad_in, out_proj, (((1,), (1,)), ((), ())), preferred_element_type=jnp.float32

time: 275 us -> 265 us (0.964)
  waiting for transfers between devices: 95.9 us -> 89.8 us
  matrix products: 44.8 us -> 39.6 us
  other arithmetic: 14 us -> 17 us
    psum x1 -> x0, waiting for transfers between devices: 49.9 us -> none  [on_device(): total = lax.psum(routed.astype(jnp.bfloat16), 'tp').astype(jnp.float32)]
    all_gather x0 -> x1, waiting for transfers between devices: none -> 22.2 us  [add_all(): parts = lax.all_gather(block, name, axis=0, tiled=False)]
    reduce_scatter x1, waiting for transfers between devices: 18.3 us -> 35.7 us  [on_device(): lax.psum_scatter(input_grad(d_gate, d_upper, gate_weight, up_weight).asty...]
    all_to_all x1, waiting for transfers between devices: 0.73 us -> 5.22 us  [on_device(): lax.all_to_all(mine.astype(jnp.bfloat16), 'sp', split_axis=1, concat_axis...]
    reduce_sum x0 -> x1, other arithmetic: none -> 3.07 us  [add_all(): acc = parts.sum(axis=0)]
where the time goes in v1:
time: 265 us; the launch traced here: 264 us
  waiting for transfers between devices  89.8 us (34%)
  local copies, waits for them, and re-layouts  62.9 us (24%)
  matrix products  39.6 us (15%)
  blocking collectives  35.8 us (14%)
  other arithmetic  17 us (6%)
  between operations  14.4 us (5%)
  starting transfers between devices  4.08 us (2%)
    reduce_scatter x1, waiting for transfers between devices, on_device(): lax.psum_scatter(input_grad(d_gate, d_upper, gate_weight, up_weight).asty...  35.7 us
    all_gather x1, waiting for transfers between devices, add_all(): parts = lax.all_gather(block, name, axis=0, tiled=False)  22.2 us
    all_gather x1, waiting for transfers between devices, on_device(): lax.all_gather(got_cot, 'tp', axis=0, tiled=True)  17.1 us
    all_gather x2, blocking collectives, entering(): everything = jax.tree.map(lambda part: lax.all_gather(part, axis), shard)  17 us
    all_to_all x1, blocking collectives, on_device(): lax.all_to_all(part_in, 'sp', split_axis=1, concat_axis=1, tiled=True)  10.7 us
    reduce_scatter x1, waiting for transfers between devices, on_device(): lax.psum_scatter(lax.dot_general(grad_in, saved_out, (((0,), (0,)), ((),...  9.57 us
    all_to_all x1, blocking collectives, on_device(): lax.all_to_all(part_cot, 'sp', split_axis=1, concat_axis=1, tiled=True)  8.11 us
    mul x3, local copies, waits for them, and re-layouts, on_device(): route_weight[:, :, None] * cotangent[:, None, :].astype(jnp.float32)  7.21 us
  transfers between devices with their start and end apart: 6, of which 5 were waited for; matrix products, arithmetic and copies ran while one was open for 25% of the time, Pallas kernels for 0%

profile of v1, /device:TPU:0, one launch (start us, length us, event | category | flops | bytes accessed | tf_op | source)
XLA Modules:
  0.0 263.9 jit_solution(9186250365814548320)
XLA Ops:
  8.5 1.2 reduce-window.6
  11.3 1.4 scatter_custom_fusion
  12.7 1.9 concatenate.6
  14.6 6.3 %gather_fusion = bf16[512,2048]{1,0:T(8,128)(2,1)} fusion(bf16[129,2048]{1,0:T(8,128)(2,1)} %concatenate.6, s32[1024]{0:T(1024)S(1)} %get-tuple-element.318), kind=kCustom, calls=%fused_computation | custom fusion | bytes 4196352 | tf_op jit(solution)/shard_map/gather | solution.py:204
  21.0 4.1 %reshape.216 = bf16[128,4,2048]{2,1,0:T(4,128)(2,1)} reshape(bf16[512,2048]{1,0:T(8,128)(2,1)} %gather_fusion) | data formatting | bytes 4194304 | tf_op jit(solution)/shard_map/reshape | solution.py:204
  25.1 1.0 constant_dynamic-slice_fusion.1
  26.3 10.7 %all_to_all.15 = bf16[16,4,2048]{2,0,1:T(8,128)(2,1)S(1)} all-to-all(bf16[16,4,2048]{2,0,1:T(8,128)(2,1)S(1)} %copy.182), channel_id=1, replica_groups=mesh['sp'=4,'tp'=8] {'sp'}, dimensions={1} | all-to-all | bytes 524288 | tf_op jit(solution)/shard_map/all_to_all | solution.py:216
  38.0 3.4 %mul.203 = f32[128,2,2048]{2,1,0:T(2,128)} broadcast(bf16[128,2048]{1,0:T(8,128)(2,1)} %param.19), dimensions={0,2} | broadcast | bytes 2621440 | tf_op jit(solution)/shard_map/mul | solution.py:199
  41.4 3.7 %mul.204 = f32[256,2048]{1,0:T(8,128)} reshape(f32[128,2,2048]{2,1,0:T(2,128)} %mul.203) | data formatting | bytes 4194304 | tf_op jit(solution)/shard_map/mul | solution.py:199
  45.3 1.9 multiply_convert_fusion
  47.2 1.1 concatenate.7
  48.3 6.6 %gather_fusion.1 = bf16[512,2048]{1,0:T(8,128)(2,1)} fusion(bf16[257,2048]{1,0:T(8,128)(2,1)} %concatenate.7, s32[1024]{0:T(1024)S(1)} %get-tuple-element.317), kind=kCustom, calls=%fused_computation.1 | custom fusion | bytes 4196352 | tf_op jit(solution)/shard_map/gather | solution.py:207
  54.9 4.1 %reshape.218 = bf16[128,4,2048]{2,1,0:T(4,128)(2,1)} reshape(bf16[512,2048]{1,0:T(8,128)(2,1)} %gather_fusion.1) | data formatting | bytes 4194304 | tf_op jit(solution)/shard_map/reshape | solution.py:207
  59.0 1.0 constant_dynamic-slice_fusion
  60.2 8.1 %all_to_all.16 = bf16[16,4,2048]{2,0,1:T(8,128)(2,1)S(1)} all-to-all(bf16[16,4,2048]{2,0,1:T(8,128)(2,1)S(1)} %copy.183), channel_id=1, replica_groups=mesh['sp'=4,'tp'=8] {'sp'}, dimensions={1} | all-to-all | bytes 524288 | tf_op jit(solution)/shard_map/all_to_all | solution.py:217
  69.5 3.9 %reshape.217 = bf16[512,2048]{1,0:T(8,128)(2,1)} reshape(bf16[128,4,2048]{2,1,0:T(4,128)(2,1)} %all-gather.8.cloned.1.call-done) | data formatting | bytes 4194304 | tf_op jit(solution)/shard_map/reshape | solution.py:224
  73.5 4.7 %fusion.3 = f32[512,768]{1,0:T(8,128)} fusion(bf16[512,2048]{1,0:T(8,128)(2,1)} %reshape.217, bf16[1,2048,768]{2,1,0:T(8,128)(2,1)S(1)} %copy-done), kind=kOutput, calls=%fused_computation.16 | convolution fusion | flops 1610612736 | bytes 6815744 | tf_op jit(solution)/shard_map/dot_general | solution.py:45
  78.2 3.0 %fusion.7 = f32[512,768]{1,0:T(8,128)} fusion(bf16[512,2048]{1,0:T(8,128)(2,1)S(1)} %copy-done.4, bf16[1,2048,768]{2,1,0:T(8,128)(2,1)S(1)} %copy-done.17), kind=kOutput, calls=%fused_computation.20 | convolution fusion | flops 1610612736 | bytes 6815744 | tf_op jit(solution)/shard_map/dot_general | solution.py:46
  81.2 17.1 %all-gather.10.cloned.1.call-done = bf16[128,4,2048]{2,1,0:T(4,128)(2,1)} async-done(((bf16[16,4,2048]{2,1,0:T(4,128)(2,1)}), bf16[128,4,2048]{2,1,0:T(4,128)(2,1)}) %all-gather.10.cloned.1.call-update) | async-done | bytes 2097168 | tf_op jit(solution)/shard_map/all_gather | solution.py:221
  98.3 3.9 %reshape.219 = bf16[512,2048]{1,0:T(8,128)(2,1)} reshape(bf16[128,4,2048]{2,1,0:T(4,128)(2,1)} %all-gather.10.cloned.1.call-done) | data formatting | bytes 4194304 | tf_op jit(solution)/shard_map/reshape | solution.py:224
  102.3 5.6 %multiply_convert_fusion.2 = (bf16[512,768]{1,0:T(8,128)(2,1)S(1)}, bf16[512,768]{1,0:T(8,128)(2,1)S(1)}) fusion(f32[512,768]{1,0:T(8,128)} %fusion.3, f32[512,768]{1,0:T(8,128)} %fusion.7, bf16[512,2048]{1,0:T(8,128)(2,1)} %reshape.219, bf16[1,768,2048]{2,1,0:T(8,128)(2,1)} %param.24), kind=kOutput, calls=%fused_computation.31 | convolution fusion | flops 1615724544 | bytes 9961472 | tf_op jit(solution)/shard_map/dot_general | solution.py:50
  107.9 1.8 fusion.1
  110.4 3.1 %add_convert_fusion = bf16[512,2048]{1,0:T(8,128)(2,1)} fusion(f32[512,2048]{1,0:T(8,128)S(1)} %fusion.1, bf16[512,768]{1,0:T(8,128)(2,1)S(1)} %get-tuple-element.305, bf16[1,2048,768]{2,1,0:T(8,128)(2,1)S(1)} %copy-done.18), kind=kOutput, calls=%fused_computation.10 | convolution fusion | flops 1612709888 | bytes 10223616 | tf_op jit(solution)/shard_map/dot_general | solution.py:73
  113.5 35.7 %reduce-scatter.3.cloned.1.call-done = bf16[64,2048]{1,0:T(8,128)(2,1)} async-done(((bf16[512,2048]{1,0:T(8,128)(2,1)}), bf16[64,2048]{1,0:T(8,128)(2,1)}) %reduce-scatter.3.cloned.1.call-update) | async-done | bytes 262160 | tf_op jit(solution)/shard_map/reduce_scatter | solution.py:227
  149.2 1.1 convert_element_type.114
  151.1 3.7 %all-to-all-start.2 = ((bf16[16,4,2048]{2,0,1:T(8,128)(2,1)}), bf16[16,4,2048]{2,0,1:T(8,128)(2,1)S(1)}, u32[]{:S(2)}, u32[]{:S(2)}) async-start(bf16[16,4,2048]{2,0,1:T(8,128)(2,1)} %copy.151), calls=%async_computation.3 | async-start | bytes 524288 | tf_op jit(solution)/shard_map/all_to_all | solution.py:237
  155.0 5.2 %all-to-all-done.2 = bf16[16,4,2048]{2,0,1:T(8,128)(2,1)S(1)} async-done(((bf16[16,4,2048]{2,0,1:T(8,128)(2,1)}), bf16[16,4,2048]{2,0,1:T(8,128)(2,1)S(1)}, u32[]{:S(2)}, u32[]{:S(2)}) %all-to-all-start.2) | async-done | bytes 262176 | tf_op jit(solution)/shard_map/all_to_all | solution.py:237
  160.6 1.5 gather_fusion.2
  162.1 2.2 gather.14
  164.3 5.7 %select_reduce_fusion = bf16[128,2048]{1,0:T(8,128)(2,1)} fusion(f32[128,2,2048]{2,1,0:T(2,128)} %gather.14, pred[128,2]{1,0:T(8,128)(4,1)S(1)} %copy.150), kind=kLoop, calls=%fused_computation.28 | loop fusion | flops 786432 | bytes 2621696 | tf_op jit(solution)/shard_map/reduce_sum | solution.py:244
  171.1 8.1 %all-gather.3 = f32[4,2,64]{2,1,0:T(2,128)S(1)} all-gather(f32[1,2,64]{2,1,0:T(2,128)S(1)} %exponential_bitcast_fusion.1), channel_id=4, replica_groups=mesh['sp'=4,'tp'=8] {'sp'}, dimensions={0}, use_global_device_ids=true | all-gather | bytes 2560 | tf_op jit(solution)/shard_map/all_gather | solution.py:19
  179.2 1.0 convolution_multiply_fusion.2
  180.2 4.7 %fusion.12 = bf16[1,2048,768]{2,1,0:T(8,128)(2,1)} fusion(bf16[512,2048]{1,0:T(8,128)(2,1)S(1)} %copy-done.5, bf16[512,768]{1,0:T(8,128)(2,1)} %copy-done.19), kind=kOutput, calls=%fused_computation.25 | convolution fusion | flops 1612185600 | bytes 6029312 | tf_op jit(solution)/shard_map/dot_general | solution.py:63
  184.9 3.5 %fusion.11 = bf16[1,2048,768]{2,1,0:T(8,128)(2,1)} fusion(bf16[512,2048]{1,0:T(8,128)(2,1)S(1)} %copy-done.5, bf16[512,768]{1,0:T(8,128)(2,1)S(1)} %copy-done.21), kind=kOutput, calls=%fused_computation.24 | convolution fusion | flops 1612185600 | bytes 6029312 | tf_op jit(solution)/shard_map/dot_general | solution.py:60
  188.5 3.6 %fusion.13 = bf16[1,768,2048]{2,1,0:T(8,128)(2,1)} fusion(bf16[512,2048]{1,0:T(8,128)(2,1)S(1)} %copy-done.6, f32[512,768]{1,0:T(8,128)S(1)} %copy-done.23, f32[512,768]{1,0:T(8,128)S(1)} %copy-done.22), kind=kOutput, calls=%fused_computation.26 | convolution fusion | flops 1614544896 | bytes 8388608 | tf_op jit(solution)/shard_map/dot_general | solution.py:57
  192.0 22.2 %all-gather.12.cloned.1.call-done = bf16[1024,2048]{1,0:T(8,128)(2,1)} async-done(((bf16[128,2048]{1,0:T(8,128)(2,1)}), bf16[1024,2048]{1,0:T(8,128)(2,1)}) %all-gather.12.cloned.1.call-update) | async-done | bytes 4194320 | tf_op jit(solution)/shard_map/all_gather | solution.py:12
  214.2 3.1 %reduce_sum.50 = bf16[128,2048]{1,0:T(8,128)(2,1)S(1)} reduce(bf16[8,128,2048]{2,1,0:T(8,128)(2,1)} %bitcast.121, bf16[]{:T(256)} %constant.131.clone.1), dimensions={0}, to_apply=%region_6.7 | reduce | flops 1835008 | bytes 4718594 | tf_op jit(solution)/shard_map/reduce_sum | solution.py:13
  218.6 8.9 %all-gather.1 = f32[8,64,128]{2,1,0:T(8,128)S(1)} all-gather(f32[2,64,128]{2,1,0:T(8,128)S(1)} %get-tuple-element.245), channel_id=3, replica_groups=mesh['sp'=4,'tp'=8] {'sp'}, dimensions={0}, use_global_device_ids=true | all-gather | bytes 327680 | tf_op jit(solution)/shard_map/all_gather | solution.py:19
  228.1 1.5 convolution_convert_fusion.3
  231.8 1.8 rev.6
  233.6 1.7 copy.175
  235.3 1.3 fusion.24
  236.7 1.0 fusion.57
  238.4 1.7 reshape.230
  240.0 1.4 convolution_multiply_fusion.1
  241.4 1.4 fusion.25
  246.0 9.6 %reduce-scatter.5.cloned.1.call-done = bf16[512,256]{1,0:T(8,128)(2,1)} async-done(((bf16[2048,256]{1,0:T(8,128)(2,1)}), bf16[512,256]{1,0:T(8,128)(2,1)}) %reduce-scatter.5.cloned.1.call-update) | async-done | bytes 262160 | tf_op jit(solution)/shard_map/reduce_scatter | solution.py:250
  255.6 1.8 convert_element_type.120
  (139 shorter events, 17.0 us)
Async XLA Ops:
  7.2 66.3 %copy-start = (bf16[1,2048,768]{2,1,0:T(8,128)(2,1)S(1)}, bf16[1,2048,768]{2,1,0:T(8,128)(2,1)}, u32[]{:S(2)}) copy-start(bf16[1,2048,768]{2,1,0:T(8,128)(2,1)} %param.22) | copy-start | bytes 9437188
  7.2 62.3 %all-gather.8.cloned.1.call-start = ((), (), s32[]{:S(2)}) async-start(), calls=%async_computation.5 | async-start | bytes 2359296 | tf_op jit(solution)/shard_map/all_gather | solution.py:220
  38.0 60.4 %all-gather.10.cloned.1.call-start = ((), (), s32[]{:S(2)}) async-start(), calls=%async_computation.6 | async-start | bytes 2359296 | tf_op jit(solution)/shard_map/all_gather | solution.py:221
  41.4 3.7 %copy-start.16 = (f32[128,2]{0,1:T(2,128)S(1)}, f32[128,2]{0,1:T(2,128)}, u32[]{:S(2)}) copy-start(f32[128,2]{0,1:T(2,128)} %param.21) | copy-start | bytes 3076
  69.3 79.9 %reduce-scatter.3.cloned.1.call-start = ((), (), s32[]{:S(2)}) async-start(), calls=%async_computation.7 | async-start | bytes 2359296 | tf_op jit(solution)/shard_map/reduce_scatter | solution.py:227
  73.5 4.7 %copy-start.4 = (bf16[512,2048]{1,0:T(8,128)(2,1)S(1)}, bf16[512,2048]{1,0:T(8,128)(2,1)}, u32[]{:S(2)}) copy-start(bf16[512,2048]{1,0:T(8,128)(2,1)} %reshape.217) | copy-start | bytes 6291460
  73.5 4.7 %copy-start.17 = (bf16[1,2048,768]{2,1,0:T(8,128)(2,1)S(1)}, bf16[1,2048,768]{2,1,0:T(8,128)(2,1)}, u32[]{:S(2)}) copy-start(bf16[1,2048,768]{2,1,0:T(8,128)(2,1)} %param.23) | copy-start | bytes 9437188
  107.9 1.9 copy-start.20
  107.9 1.9 copy-start.19
  107.9 2.5 copy-start.18
  151.1 9.1 %all-to-all-start.2 = ((bf16[16,4,2048]{2,0,1:T(8,128)(2,1)}), bf16[16,4,2048]{2,0,1:T(8,128)(2,1)S(1)}, u32[]{:S(2)}, u32[]{:S(2)}) async-start(bf16[16,4,2048]{2,0,1:T(8,128)(2,1)} %copy.151), calls=%async_computation.3 | async-start | bytes 524288 | tf_op jit(solution)/shard_map/all_to_all | solution.py:237
  154.8 59.4 %all-gather.12.cloned.1.call-start = ((), (), s32[]{:S(2)}) async-start(), calls=%async_computation.9 | async-start | bytes 4718592 | tf_op jit(solution)/shard_map/all_gather | solution.py:12
  164.3 5.9 %copy-start.11 = (f32[128,128]{1,0:T(8,128)S(1)}, f32[128,128]{1,0:T(8,128)}, u32[]{:S(2)}) copy-start(f32[128,128]{1,0:T(8,128)} %param.30) | copy-start | bytes 196612
  164.3 6.2 %copy-start.14 = (bf16[128,128]{1,0:T(8,128)(2,1)S(1)}, bf16[128,128]{1,0:T(8,128)(2,1)}, u32[]{:S(2)}) copy-start(bf16[128,128]{1,0:T(8,128)(2,1)} %param.27) | copy-start | bytes 98308
  164.3 6.4 %copy-start.15 = (bf16[128,128]{1,0:T(8,128)(2,1)S(1)}, bf16[128,128]{1,0:T(8,128)(2,1)}, u32[]{:S(2)}) copy-start(bf16[128,128]{1,0:T(8,128)(2,1)} %param.28) | copy-start | bytes 98308
  164.3 6.7 %copy-start.13 = (bf16[128,256]{1,0:T(8,128)(2,1)S(1)}, bf16[128,256]{1,0:T(8,128)(2,1)}, u32[]{:S(2)}) copy-start(bf16[128,256]{1,0:T(8,128)(2,1)} %param.29) | copy-start | bytes 196612
  170.1 10.1 %copy-start.5 = (bf16[512,2048]{1,0:T(8,128)(2,1)S(1)}, bf16[512,2048]{1,0:T(8,128)(2,1)}, u32[]{:S(2)}) copy-start(bf16[512,2048]{1,0:T(8,128)(2,1)} %reshape.217) | copy-start | bytes 6291460
  170.1 85.5 %reduce-scatter.5.cloned.1.call-start = ((), (), s32[]{:S(2)}) async-start(), calls=%async_computation.8 | async-start | bytes 1310720 | tf_op jit(solution)/shard_map/reduce_scatter | solution.py:250
  180.2 4.7 %copy-start.21 = (bf16[512,768]{1,0:T(8,128)(2,1)S(1)}, bf16[512,768]{1,0:T(8,128)(2,1)}, u32[]{:S(2)}) copy-start(bf16[512,768]{1,0:T(8,128)(2,1)} %copy-done.20) | copy-start | bytes 2359300
  184.9 3.5 %copy-start.6 = (bf16[512,2048]{1,0:T(8,128)(2,1)S(1)}, bf16[512,2048]{1,0:T(8,128)(2,1)}, u32[]{:S(2)}) copy-start(bf16[512,2048]{1,0:T(8,128)(2,1)} %reshape.219) | copy-start | bytes 6291460
  184.9 3.5 %copy-start.22 = (f32[512,768]{1,0:T(8,128)S(1)}, f32[512,768]{1,0:T(8,128)}, u32[]{:S(2)}) copy-start(f32[512,768]{1,0:T(8,128)} %fusion.3) | copy-start | bytes 4718596
  184.9 3.5 %copy-start.23 = (f32[512,768]{1,0:T(8,128)S(1)}, f32[512,768]{1,0:T(8,128)}, u32[]{:S(2)}) copy-start(f32[512,768]{1,0:T(8,128)} %fusion.7) | copy-start | bytes 4718596
  214.2 3.1 %copy-start.2 = (bf16[128,2048]{1,0:T(8,128)(2,1)S(1)}, bf16[128,2048]{1,0:T(8,128)(2,1)}, u32[]{:S(2)}) copy-start(bf16[128,2048]{1,0:T(8,128)(2,1)} %param.19) | copy-start | bytes 1572868
  214.2 3.1 %copy-start.8 = (bf16[256,2048]{1,0:T(8,128)(2,1)S(1)}, bf16[256,2048]{1,0:T(8,128)(2,1)}, u32[]{:S(2)}) copy-start(bf16[256,2048]{1,0:T(8,128)(2,1)} %param.25) | copy-start | bytes 3145732
  217.8 10.3 %copy-start.12 = (bf16[128,256]{1,0:T(8,128)(2,1)S(1)}, bf16[128,256]{1,0:T(8,128)(2,1)}, u32[]{:S(2)}) copy-start(bf16[128,256]{1,0:T(8,128)(2,1)} %param.26) | copy-start | bytes 196612
  217.9 11.9 %copy-start.3 = (f32[2,64,2,128]{3,2,1,0:T(2,128)}, f32[2,64,2,128]{3,2,1,0:T(2,128)S(1)}, u32[]{:S(2)}) copy-start(f32[2,64,2,128]{3,2,1,0:T(2,128)S(1)} %reshape.225) | copy-start | bytes 393220
  218.5 11.6 %copy-start.7 = (f32[2,2,64,128]{3,2,1,0:T(8,128)}, f32[2,2,64,128]{3,2,1,0:T(8,128)S(1)}, u32[]{:S(2)}) copy-start(f32[2,2,64,128]{3,2,1,0:T(8,128)S(1)} %get-tuple-element.244) | copy-start | bytes 393220
  228.1 1.7 copy-start.9
  231.8 25.5 %copy-start.1 = (bf16[1,2048,768]{2,1,0:T(8,128)(2,1)S(1)}, bf16[1,2048,768]{2,1,0:T(8,128)(2,1)}, u32[]{:S(2)}) copy-start(bf16[1,2048,768]{2,1,0:T(8,128)(2,1)} %param.22) | copy-start | bytes 9437188
  236.6 8.5 %copy-start.10 = (bf16[2,64,2,64]{1,3,2,0:T(8,128)(2,1)S(1)}, bf16[2,64,2,64]{1,3,2,0:T(8,128)(2,1)}, u32[]{:S(2)}) copy-start(bf16[2,64,2,64]{1,3,2,0:T(8,128)(2,1)} %get-tuple-element.309) | copy-start | bytes 98308
Sparse Core Ops, SparseCore 0:
  38.1 28.8 all-gather.7
  69.4 28.8 all-gather.9
  113.7 35.4 reduce-scatter.2
  170.2 43.9 all-gather.11
  229.7 25.8 reduce-scatter.4
